TPU v7x, 32 devices: a whole 2x2x4 slice. The times are simulated.
32 devices in a mesh: sp: 16 (over z, y, x), tp: 2 (over core).
Axes of the slice: x: 2, y: 2, z: 4, core: 2. Of those that a mesh axis runs over, the one named last changes fastest.
Arguments:
- stream: bfloat16 [6144, 2048], P('sp'), may hold values from -40 to 40
- query_rows: bfloat16 [6144, 1024], P('sp', 'tp'), may hold values from -10 to 10
- key_rows: bfloat16 [6144, 256], P('sp'), may hold values from -10 to 10
- value_rows: bfloat16 [6144, 256], P('sp'), may hold values from -6 to 6
- doc_ids: int32 [6144], P('sp'), may hold values from 0 to 7, never falling along the last dimension, each value on 1 to 1536 neighbouring positions
- sink_logit: float32 [8], P('tp'), may hold values from 2 to 7
- out_weight: bfloat16 [1024, 2048], P('tp'), may hold values from -1.5 to 1.5
- norm_gain: float32 [2048], replicated, may hold values from 0.1 to 1.9
- gate_weight: bfloat16 [2048, 5632], P('sp', 'tp'), may hold values from -0.125 to 0.125
- up_weight: bfloat16 [2048, 5632], P('sp', 'tp'), may hold values from -0.125 to 0.125
- down_weight: bfloat16 [5632, 2048], P('tp', 'sp'), may hold values from -0.078125 to 0.078125
Outputs:
- mixed_out: bfloat16 [6144, 2048], P('sp')
Inputs may be any that keep to these rules, and one draw needn't show every extreme that they name: `doc_ids`: document numbers never fall along the sequence; each document has 1 to 1536 positions.
All inputs are finite; a program needn't handle non-finite values.
Results may differ from a plain program's by a relative error of at most 0.009.
Values may be sent and summed in bfloat16 or wider, within the bound.
No kernel may reach another device: no remote copies, remote signals or barrier semaphores. Data moves between devices by JAX's collectives and lax.ppermute only.
A program may use at most 128 MiB of HBM per device.

v0:
```python
import jax
import jax.numpy as jnp
from jax import lax
from jax.sharding import PartitionSpec as P

HEADS = 8
KVH = 2
HD = 128
WIN = 128
norm_eps = 1e-06
masked_low = -1e30


def extended(value, sides, width):
    for axis, dim in sides:
        peers, length = (lax.axis_size(axis), value.shape[dim])
        up = [(i, (i + 1) % peers) for i in range(peers - 1)]
        down = [(j, i) for i, j in up]
        last = lax.slice_in_dim(value, length - width, length, axis=dim)
        initial = lax.slice_in_dim(value, 0, width, axis=dim)
        before = lax.ppermute(last, axis, up)
        after = lax.ppermute(initial, axis, down)
        value = jnp.concatenate([before, value, after], axis=dim)
    return value


def per_device(
    stream,
    query_rows,
    key_rows,
    value_rows,
    doc_ids,
    sink_logit,
    out_weight,
    norm_gain,
    gate_weight,
    up_weight,
    down_weight,
):
    row_count = stream.shape[0]
    heads_here = query_rows.shape[1] // HD
    group_share = HEADS // KVH
    groups_here = max(1, heads_here // group_share)
    per_group = heads_here // groups_here
    tp_place = lax.axis_index("tp")
    group_first = tp_place * heads_here // group_share
    keys_here = lax.dynamic_slice_in_dim(key_rows, group_first * HD, groups_here * HD, 1)
    values_here = lax.dynamic_slice_in_dim(value_rows, group_first * HD, groups_here * HD, 1)
    keys_wide, values_wide, docs_wide = (
        extended(keys_here, (("sp", 0),), WIN),
        extended(values_here, (("sp", 0),), WIN),
        extended(doc_ids, (("sp", 0),), WIN),
    )
    seq_offset = lax.axis_index("sp") * row_count
    seq_total = row_count * lax.axis_size("sp")
    query_pos = seq_offset + jnp.arange(row_count, dtype=jnp.int32)
    key_pos = seq_offset - WIN + jnp.arange(row_count + 2 * WIN, dtype=jnp.int32)
    allowed = (
        (jnp.abs(query_pos[:, None] - key_pos[None, :]) <= WIN)
        & (key_pos[None, :] >= 0)
        & (key_pos[None, :] < seq_total)
        & (doc_ids[:, None] == docs_wide[None, :])
    )
    queries = query_rows.reshape(row_count, groups_here, per_group, HD)
    keys_grid = keys_wide.reshape(row_count + 2 * WIN, groups_here, HD)
    values_grid = values_wide.reshape(row_count + 2 * WIN, groups_here, HD)
    scores = jnp.einsum(
        "qgrd,kgd->grqk", queries, keys_grid, preferred_element_type=jnp.float32
    ) * HD ** (-0.5)
    masked = jnp.where(allowed[None, None], scores, masked_low)
    sinks = sink_logit.reshape(groups_here, per_group, 1, 1)
    peak = jnp.maximum(jnp.max(masked, axis=-1, keepdims=True), sinks)
    lifted = jnp.where(allowed[None, None], jnp.exp(masked - peak), 0.0)
    denom = jnp.sum(lifted, axis=-1, keepdims=True) + jnp.exp(sinks - peak)
    probs = (lifted / denom).astype(jnp.bfloat16)
    attended = jnp.einsum("grqk,kgd->qgrd", probs, values_grid, preferred_element_type=jnp.float32)
    attended = attended.astype(jnp.bfloat16).reshape(row_count, heads_here * HD)
    partial_value = jnp.dot(attended, out_weight, preferred_element_type=jnp.float32)
    branch = lax.psum(partial_value.astype(jnp.bfloat16), "tp")
    carried = (stream.astype(jnp.float32) + branch.astype(jnp.float32)).astype(jnp.bfloat16)
    carried_f = carried.astype(jnp.float32)
    normed = (
        carried_f
        * lax.rsqrt(jnp.mean(carried_f * carried_f, axis=1, keepdims=True) + norm_eps)
        * norm_gain[None, :]
    ).astype(jnp.bfloat16)

    def add_rows(weight_rows):
        return jnp.dot(normed, weight_rows, preferred_element_type=jnp.float32)

    gate_acc = add_rows(lax.all_gather(gate_weight, "sp", axis=0, tiled=True))
    up_acc = add_rows(lax.all_gather(up_weight, "sp", axis=0, tiled=True))
    hidden = (jax.nn.silu(gate_acc) * up_acc).astype(jnp.bfloat16)
    terms = jnp.dot(
        hidden,
        lax.all_gather(down_weight, "sp", axis=1, tiled=True),
        preferred_element_type=jnp.float32,
    )
    feed = lax.psum(terms.astype(jnp.bfloat16), "tp")
    return (carried_f + 0.5 * feed.astype(jnp.float32)).astype(jnp.bfloat16)


def solution(mesh):
    in_specs = (
        P("sp", None),
        P("sp", "tp"),
        P("sp", None),
        P("sp", None),
        P("sp"),
        P("tp"),
        P("tp", None),
        P(),
        P("sp", "tp"),
        P("sp", "tp"),
        P("tp", "sp"),
    )
    out_specs = P("sp", None)
    return jax.shard_map(
        per_device, mesh=mesh, in_specs=in_specs, out_specs=out_specs, check_vma=False
    )
```

profile of v0, /device:TPU:0, one launch (start us, length us, event | category | flops | bytes accessed | tf_op | source)
XLA Modules:
  0.0 561.7 jit_solution(12022949672108720570)
XLA Ops:
  7.4 0.0 copy-start
  7.4 0.0 copy-start.1
  7.4 0.0 all-reduce.3.cloned.1.call-start
  7.4 0.9 fusion.38
  8.3 4.9 collective-permute-start.4
  13.2 1.3 collective-permute-start.5
  14.5 0.8 fusion.40
  15.2 4.5 collective-permute-start.2
  19.8 1.3 collective-permute-start.3
  21.1 1.0 constant_dynamic-slice_fusion.1
  22.1 0.1 copy.16
  22.2 4.9 collective-permute-start
  27.2 0.0 collective-permute-done.2
  27.2 1.3 collective-permute-start.1
  28.5 0.0 collective-permute-done.3
  28.5 0.7 pad_add_fusion
  29.2 1.4 fusion.14
  30.6 0.0 collective-permute-done.4
  30.6 0.0 collective-permute-done.5
  30.6 1.8 fusion.1
  32.4 0.0 copy-done.1
  32.4 0.1 broadcast_maximum_fusion
  32.5 1.0 fusion.6
  33.5 0.1 exponential_add_fusion
  33.6 0.0 collective-permute-done
  33.6 0.3 collective-permute-done.1
  33.9 1.5 fusion.9
  35.4 0.0 copy-done
  35.4 2.2 convolution_convert_fusion.1
  37.6 0.0 copy-start.2
  37.6 0.0 all-reduce.3.cloned.1.call-update
  37.6 0.0 all-gather.4.cloned.1.call-start
  37.6 0.5 all-gather.4.cloned.1.call-update
  38.2 0.0 all-gather.6.cloned.1.call-start
  38.2 0.5 all-gather.6.cloned.1.call-update
  38.8 0.0 all-gather.8.cloned.1.call-start
  38.8 0.5 all-gather.8.cloned.1.call-update
  39.3 0.2 all-reduce.5.cloned.1.call-start
  39.6 23.8 %all-reduce.3.cloned.1.call-done = bf16[384,2048]{1,0:T(8,128)(2,1)} async-done(((bf16[384,2048]{1,0:T(8,128)(2,1)}), bf16[384,2048]{1,0:T(8,128)(2,1)}) %all-reduce.3.cloned.1.call-update) | async-done | bytes 1572880 | tf_op jit(solution)/shard_map/psum | solution.py:79
  63.3 3.6 fusion.2
  66.9 120.3 %all-gather.4.cloned.1.call-done = bf16[2048,2816]{1,0:T(8,128)(2,1)} async-done(((bf16[128,2816]{1,0:T(8,128)(2,1)}), bf16[2048,2816]{1,0:T(8,128)(2,1)}) %all-gather.4.cloned.1.call-update) | async-done | bytes 11534352 | tf_op jit(solution)/shard_map/all_gather | solution.py:91
  187.2 0.0 copy-done.2
  187.2 11.5 %fusion.17 = f32[384,2816]{1,0:T(8,128)} fusion(bf16[2048,2816]{1,0:T(8,128)(2,1)} %all-gather.4.cloned.1.call-done, bf16[384,2048]{1,0:T(8,128)(2,1)} %get-tuple-element.6, f32[2048]{0:T(1024)S(1)} %copy-done.2, f32[384]{0:T(512)S(1)} %add_rsqrt_fusion), kind=kOutput, calls=%fused_computation.24 | convolution fusion | flops 4432330752 | bytes 17442304 | tf_op jit(solution)/shard_map/dot_general | solution.py:89
  198.8 130.5 %all-gather.6.cloned.1.call-done = bf16[2048,2816]{1,0:T(8,128)(2,1)} async-done(((bf16[128,2816]{1,0:T(8,128)(2,1)}), bf16[2048,2816]{1,0:T(8,128)(2,1)}) %all-gather.6.cloned.1.call-update) | async-done | bytes 11534352 | tf_op jit(solution)/shard_map/all_gather | solution.py:92
  329.3 182.7 %all-gather.8.cloned.1.call-done = bf16[2816,2048]{1,0:T(8,128)(2,1)} async-done(((bf16[2816,128]{1,0:T(8,128)(2,1)}), bf16[2816,2048]{1,0:T(8,128)(2,1)}) %all-gather.8.cloned.1.call-update) | async-done | bytes 11534352 | tf_op jit(solution)/shard_map/all_gather | solution.py:96
  511.9 19.8 %convolution_convert_fusion = bf16[384,2048]{1,0:T(8,128)(2,1)} fusion(bf16[2816,2048]{1,0:T(8,128)(2,1)} %all-gather.8.cloned.1.call-done, bf16[2048,2816]{1,0:T(8,128)(2,1)} %all-gather.6.cloned.1.call-done, f32[384,2816]{1,0:T(8,128)} %fusion.17, bf16[384,2048]{1,0:T(8,128)(2,1)} %get-tuple-element.6, f32[2048]{0:T(1024)S(1)} %copy-done.2, ...), kind=kOutput, calls=%fused_computation.14 | convolution fusion | flops 8868790272 | bytes 30549504 | tf_op jit(solution)/shard_map/dot_general | solution.py:94
  531.7 0.0 all-reduce.5.cloned.1.call-update
  531.7 18.7 %all-reduce.5.cloned.1.call-done = bf16[384,2048]{1,0:T(8,128)(2,1)} async-done(((bf16[384,2048]{1,0:T(8,128)(2,1)}), bf16[384,2048]{1,0:T(8,128)(2,1)}) %all-reduce.5.cloned.1.call-update) | async-done | bytes 1572880 | tf_op jit(solution)/shard_map/psum | solution.py:99
  550.5 3.7 fusion.5
  (5 shorter events, 0.0 us)
Async XLA Ops:
  7.4 28.0 %copy-start = (bf16[512,2048]{1,0:T(8,128)(2,1)S(1)}, bf16[512,2048]{1,0:T(8,128)(2,1)}, u32[]{:S(2)}) copy-start(bf16[512,2048]{1,0:T(8,128)(2,1)} %param.17) | copy-start | bytes 6291460
  7.4 25.1 %copy-start.1 = (f32[4]{0:T(128)S(1)}, f32[4]{0:T(128)}, u32[]{:S(2)}) copy-start(f32[4]{0:T(128)} %param.16) | copy-start | bytes 52
  7.4 56.0 %all-reduce.3.cloned.1.call-start = ((), (), s32[]{:S(2)}) async-start(), calls=%async_computation | async-start | bytes 3145728 | tf_op jit(solution)/shard_map/psum | solution.py:79
  8.3 22.3 %collective-permute-start.4 = (bf16[128,128]{1,0:T(8,128)(2,1)S(1)}, bf16[128,128]{1,0:T(8,128)(2,1)S(1)}, u32[]{:S(2)}, u32[]{:S(2)}) collective-permute-start(bf16[128,128]{1,0:T(8,128)(2,1)S(1)} %get-tuple-element.7), channel_id=1, source_target_pairs={{0,2},{2,4},{4,6},{6,8},{8,10},{10,12},{12,14},{14,16},{16,18},{18... | collective-permute-start | bytes 98312 | tf_op jit(solution)/shard_map/ppermute | solution.py:21
  13.2 17.4 %collective-permute-start.5 = (bf16[128,128]{1,0:T(8,128)(2,1)S(1)}, bf16[128,128]{1,0:T(8,128)(2,1)S(1)}, u32[]{:S(2)}, u32[]{:S(2)}) collective-permute-start(bf16[128,128]{1,0:T(8,128)(2,1)S(1)} %get-tuple-element.8), channel_id=1, source_target_pairs={{2,0},{4,2},{6,4},{8,6},{10,8},{12,10},{14,12},{16,14},{18,16},{20... | collective-permute-start | bytes 98312 | tf_op jit(solution)/shard_map/ppermute | solution.py:22
  15.2 11.9 %collective-permute-start.2 = (s32[128]{0:T(128)S(1)}, s32[128]{0:T(128)S(1)}, u32[]{:S(2)}, u32[]{:S(2)}) collective-permute-start(s32[128]{0:T(128)S(1)} %get-tuple-element.11), channel_id=1, source_target_pairs={{0,2},{2,4},{4,6},{6,8},{8,10},{10,12},{12,14},{14,16},{16,18},{18... | collective-permute-start | bytes 1544 | tf_op jit(solution)/shard_map/ppermute | solution.py:21
  19.8 8.7 %collective-permute-start.3 = (s32[128]{0:T(128)S(1)}, s32[128]{0:T(128)S(1)}, u32[]{:S(2)}, u32[]{:S(2)}) collective-permute-start(s32[128]{0:T(128)S(1)} %get-tuple-element.12), channel_id=1, source_target_pairs={{2,0},{4,2},{6,4},{8,6},{10,8},{12,10},{14,12},{16,14},{18,16},{20... | collective-permute-start | bytes 1544 | tf_op jit(solution)/shard_map/ppermute | solution.py:22
  22.2 11.4 %collective-permute-start = (bf16[128,128]{0,1:T(8,128)(2,1)S(1)}, bf16[128,128]{0,1:T(8,128)(2,1)S(1)}, u32[]{:S(2)}, u32[]{:S(2)}) collective-permute-start(bf16[128,128]{0,1:T(8,128)(2,1)S(1)} %get-tuple-element.9), channel_id=1, source_target_pairs={{0,2},{2,4},{4,6},{6,8},{8,10},{10,12},{12,14},{14,16},{16,18},{18... | collective-permute-start | bytes 98312 | tf_op jit(solution)/shard_map/ppermute | solution.py:21
  27.2 6.7 %collective-permute-start.1 = (bf16[128,128]{0,1:T(8,128)(2,1)S(1)}, bf16[128,128]{0,1:T(8,128)(2,1)S(1)}, u32[]{:S(2)}, u32[]{:S(2)}) collective-permute-start(bf16[128,128]{0,1:T(8,128)(2,1)S(1)} %get-tuple-element.10), channel_id=1, source_target_pairs={{2,0},{4,2},{6,4},{8,6},{10,8},{12,10},{14,12},{16,14},{18,16},{20... | collective-permute-start | bytes 98312 | tf_op jit(solution)/shard_map/ppermute | solution.py:22
  37.6 149.7 %copy-start.2 = (f32[2048]{0:T(1024)S(1)}, f32[2048]{0:T(1024)}, u32[]{:S(2)}) copy-start(f32[2048]{0:T(1024)} %param.18) | copy-start | bytes 24580
  37.6 149.7 %all-gather.4.cloned.1.call-start = ((), (), s32[]{:S(2)}) async-start(), calls=%async_computation.1 | async-start | bytes 12255232 | tf_op jit(solution)/shard_map/all_gather | solution.py:91
  38.2 291.1 %all-gather.6.cloned.1.call-start = ((), (), s32[]{:S(2)}) async-start(), calls=%async_computation.2 | async-start | bytes 12255232 | tf_op jit(solution)/shard_map/all_gather | solution.py:92
  38.8 473.2 %all-gather.8.cloned.1.call-start = ((), (), s32[]{:S(2)}) async-start(), calls=%async_computation.3 | async-start | bytes 12255232 | tf_op jit(solution)/shard_map/all_gather | solution.py:96
  39.3 511.1 %all-reduce.5.cloned.1.call-start = ((), (), s32[]{:S(2)}) async-start(), calls=%async_computation.4 | async-start | bytes 3145728 | tf_op jit(solution)/shard_map/psum | solution.py:99
Sparse Core Ops, SparseCore 0:
  37.7 25.5 all-reduce.2
  531.9 18.5 all-reduce.4
Sparse Core Ops, SparseCore 1:
  40.8 146.4 all-gather.3
  189.9 139.3 all-gather.5
  331.8 180.0 all-gather.7
where the time goes:
time: 562 us
  waiting for transfers between devices  478 us (85%)
  matrix products  36.8 us (7%)
  starting transfers between devices  18.6 us (3%)
  between operations  15.2 us (3%)
  other arithmetic  10.5 us (2%)
    all_gather x1, waiting for transfers between devices, per_device(): lax.all_gather(down_weight, 'sp', axis=1, tiled=True)  183 us
    all_gather x1, waiting for transfers between devices, per_device(): up_acc = add_rows(lax.all_gather(up_weight, 'sp', axis=0, tiled=True))  130 us
    all_gather x1, waiting for transfers between devices, per_device(): gate_acc = add_rows(lax.all_gather(gate_weight, 'sp', axis=0, tiled=True))  120 us
    psum x1, waiting for transfers between devices, per_device(): branch = lax.psum(partial_value.astype(jnp.bfloat16), 'tp')  23.8 us
    dot_general x1, matrix products, per_device(): jnp.dot(hidden, lax.all_gather(down_weight, 'sp', axis=1, tiled=True), pr...  19.8 us
    psum x1, waiting for transfers between devices, per_device(): feed = lax.psum(terms.astype(jnp.bfloat16), 'tp')  18.7 us
    ppermute x3, starting transfers between devices, extended(): before = lax.ppermute(last, axis, up)  14.3 us
    dot_general x1, matrix products, add_rows(): return jnp.dot(normed, weight_rows, preferred_element_type=jnp.float32)  11.5 us
  transfers between devices with their start and end apart: 11, of which 6 were waited for; matrix products, arithmetic and copies ran while one was open for 4% of the time, Pallas kernels for 0%

commit v1 on v0

--- a/solution.py
+++ b/solution.py
@@ -9,6 +9,11 @@
 WIN = 128
 norm_eps = 1e-06
 masked_low = -1e30
+
+
+def gathered_along(x, mesh_axis, dim):
+    parts = lax.all_gather(x, mesh_axis)
+    return jnp.concatenate(parts, axis=dim)
 
 
 def extended(value, sides, width):
@@ -92,9 +97,7 @@
     up_acc = add_rows(lax.all_gather(up_weight, "sp", axis=0, tiled=True))
     hidden = (jax.nn.silu(gate_acc) * up_acc).astype(jnp.bfloat16)
     terms = jnp.dot(
-        hidden,
-        lax.all_gather(down_weight, "sp", axis=1, tiled=True),
-        preferred_element_type=jnp.float32,
+        hidden, gathered_along(down_weight, "sp", 1), preferred_element_type=jnp.float32
     )
     feed = lax.psum(terms.astype(jnp.bfloat16), "tp")
     return (carried_f + 0.5 * feed.astype(jnp.float32)).astype(jnp.bfloat16)

time: 562 us -> 524 us (0.932)
  waiting for transfers between devices: 478 us -> 425 us
  local copies, waits for them, and re-layouts: 2.81 us -> 18 us
    all_gather x1, waiting for transfers between devices: 183 us -> 121 us  [gathered_along(): parts = lax.all_gather(x, mesh_axis)]
    reshape x0 -> x1, local copies, waits for them, and re-layouts: none -> 15.2 us  [gathered_along(): return jnp.concatenate(parts, axis=dim)]
    all_gather x1, waiting for transfers between devices: 120 us -> 127 us  [per_device(): gate_acc = add_rows(lax.all_gather(gate_weight, 'sp', axis=0, tiled=True))]
  transfers between devices with their start and end apart: 11 -> 11, of which waited for: 6 -> 6; matrix products, arithmetic and copies ran while one was open for 4% -> 7% of each run, Pallas kernels for 0% -> 0%
where the time goes in v1:
time: 524 us; the launch traced here: 523 us
  waiting for transfers between devices  425 us (81%)
  matrix products  37 us (7%)
  starting transfers between devices  18.6 us (4%)
  local copies, waits for them, and re-layouts  18 us (3%)
  between operations  15.2 us (3%)
  other arithmetic  9.58 us (2%)
    all_gather x1, waiting for transfers between devices, per_device(): up_acc = add_rows(lax.all_gather(up_weight, 'sp', axis=0, tiled=True))  132 us
    all_gather x1, waiting for transfers between devices, per_device(): gate_acc = add_rows(lax.all_gather(gate_weight, 'sp', axis=0, tiled=True))  127 us
    all_gather x1, waiting for transfers between devices, gathered_along(): parts = lax.all_gather(x, mesh_axis)  121 us
    psum x1, waiting for transfers between devices, per_device(): branch = lax.psum(partial_value.astype(jnp.bfloat16), 'tp')  23.8 us
    dot_general x1, matrix products, per_device(): jnp.dot(hidden, gathered_along(down_weight, 'sp', 1), preferred_element_t...  21.9 us
    psum x1, waiting for transfers between devices, per_device(): feed = lax.psum(terms.astype(jnp.bfloat16), 'tp')  18.7 us
    reshape x1, local copies, waits for them, and re-layouts, gathered_along(): return jnp.concatenate(parts, axis=dim)  15.2 us
    ppermute x3, starting transfers between devices, extended(): before = lax.ppermute(last, axis, up)  14.3 us
  transfers between devices with their start and end apart: 11, of which 6 were waited for; matrix products, arithmetic and copies ran while one was open for 7% of the time, Pallas kernels for 0%

profile of v1, /device:TPU:0, one launch (start us, length us, event | category | flops | bytes accessed | tf_op | source)
XLA Modules:
  0.0 523.2 jit_solution(14674159017082361998)
XLA Ops:
  7.4 0.0 copy-start
  7.4 0.0 copy-start.3
  7.4 0.0 all-reduce.3.cloned.1.call-start
  7.4 0.9 fusion.38
  8.3 4.9 collective-permute-start.4
  13.2 1.3 collective-permute-start.5
  14.5 0.8 fusion.40
  15.2 4.5 collective-permute-start.2
  19.8 1.3 collective-permute-start.3
  21.1 1.0 constant_dynamic-slice_fusion.1
  22.1 0.1 copy.23
  22.2 4.9 collective-permute-start
  27.2 0.0 collective-permute-done.2
  27.2 1.3 collective-permute-start.1
  28.5 0.0 collective-permute-done.3
  28.5 0.7 pad_add_fusion
  29.2 1.4 fusion.14
  30.6 0.0 collective-permute-done.4
  30.6 0.0 collective-permute-done.5
  30.6 1.8 fusion.1
  32.4 0.0 copy-done.3
  32.4 0.1 broadcast_maximum_fusion
  32.5 1.0 fusion.6
  33.5 0.1 exponential_add_fusion
  33.6 0.0 collective-permute-done
  33.6 0.3 collective-permute-done.1
  33.9 1.5 fusion.9
  35.4 0.0 copy-done
  35.4 2.2 convolution_convert_fusion.1
  37.6 0.0 all-reduce.3.cloned.1.call-update
  37.6 0.0 all-gather.9.cloned.1.call-start
  37.6 0.5 all-gather.9.cloned.1.call-update
  38.2 0.0 all-gather.5.cloned.1.call-start
  38.2 0.5 all-gather.5.cloned.1.call-update
  38.7 0.0 all-gather.7.cloned.1.call-start
  38.8 0.5 all-gather.7.cloned.1.call-update
  39.3 0.2 all-reduce.5.cloned.1.call-start
  39.6 23.8 %all-reduce.3.cloned.1.call-done = bf16[384,2048]{1,0:T(8,128)(2,1)} async-done(((bf16[384,2048]{1,0:T(8,128)(2,1)}), bf16[384,2048]{1,0:T(8,128)(2,1)}) %all-reduce.3.cloned.1.call-update) | async-done | bytes 1572880 | tf_op jit(solution)/shard_map/psum | solution.py:84
  63.3 2.6 fusion.2
  66.0 0.0 copy-start.2
  66.0 121.3 %all-gather.9.cloned.1.call-done = bf16[45056,128]{1,0:T(8,128)(2,1)} async-done(((bf16[2816,128]{1,0:T(8,128)(2,1)}), bf16[45056,128]{1,0:T(8,128)(2,1)}) %all-gather.9.cloned.1.call-update) | async-done | bytes 11534352 | tf_op jit(solution)/shard_map/all_gather | solution.py:15
  187.2 0.0 copy-start.4
  187.2 15.2 %copy.21 = bf16[2816,16,128]{0,2,1:T(8,128)(2,1)} copy(bf16[2816,16,128]{2,0,1:T(8,128)(2,1)} %bitcast.53) | data formatting | bytes 23068672 | tf_op jit(solution)/shard_map/reshape | solution.py:16
  202.5 126.8 %all-gather.5.cloned.1.call-done = bf16[2048,2816]{1,0:T(8,128)(2,1)} async-done(((bf16[128,2816]{1,0:T(8,128)(2,1)}), bf16[2048,2816]{1,0:T(8,128)(2,1)}) %all-gather.5.cloned.1.call-update) | async-done | bytes 11534352 | tf_op jit(solution)/shard_map/all_gather | solution.py:96
  329.3 0.0 copy-done.2
  329.3 0.0 copy-done.4
  329.3 9.7 %fusion.17 = f32[384,2816]{1,0:T(8,128)} fusion(bf16[2048,2816]{1,0:T(8,128)(2,1)} %all-gather.5.cloned.1.call-done, bf16[384,2048]{1,0:T(8,128)(2,1)S(1)} %get-tuple-element.6, f32[2048]{0:T(1024)S(1)} %copy-done.4, f32[384]{0:T(512)S(1)} %add_rsqrt_fusion), kind=kOutput, calls=%fused_computation.24 | convolution fusion | flops 4432330752 | bytes 17442304 | tf_op jit(solution)/shard_map/dot_general | solution.py:94
  338.9 132.3 %all-gather.7.cloned.1.call-done = bf16[2048,2816]{1,0:T(8,128)(2,1)} async-done(((bf16[128,2816]{1,0:T(8,128)(2,1)}), bf16[2048,2816]{1,0:T(8,128)(2,1)}) %all-gather.7.cloned.1.call-update) | async-done | bytes 11534352 | tf_op jit(solution)/shard_map/all_gather | solution.py:97
  471.3 0.0 copy-start.1
  471.3 21.9 %convolution_convert_fusion = bf16[384,2048]{1,0:T(8,128)(2,1)} fusion(bf16[2816,2048]{0,1:T(8,128)(2,1)} %bitcast.54, bf16[2048,2816]{1,0:T(8,128)(2,1)} %all-gather.7.cloned.1.call-done, f32[384,2816]{1,0:T(8,128)} %fusion.17, bf16[384,2048]{1,0:T(8,128)(2,1)} %copy-done.2, f32[2048]{0:T(1024)S(1)} %copy-done.4, f32[384]{0:T(512)S(1)} %add_rsqrt_fusion), kind=kOutput, calls=%fused_computation.14 | convolution fusion | flops 8868790272 | bytes 30549504 | tf_op jit(solution)/shard_map/dot_general | solution.py:99
  493.2 0.0 all-reduce.5.cloned.1.call-update
  493.2 18.7 %all-reduce.5.cloned.1.call-done = bf16[384,2048]{1,0:T(8,128)(2,1)} async-done(((bf16[384,2048]{1,0:T(8,128)(2,1)}), bf16[384,2048]{1,0:T(8,128)(2,1)}) %all-reduce.5.cloned.1.call-update) | async-done | bytes 1572880 | tf_op jit(solution)/shard_map/psum | solution.py:102
  511.9 3.7 fusion.5
  515.6 0.0 copy-done.1
  (5 shorter events, 0.0 us)
Async XLA Ops:
  7.4 28.0 %copy-start = (bf16[512,2048]{1,0:T(8,128)(2,1)S(1)}, bf16[512,2048]{1,0:T(8,128)(2,1)}, u32[]{:S(2)}) copy-start(bf16[512,2048]{1,0:T(8,128)(2,1)} %param.17) | copy-start | bytes 6291460
  7.4 25.1 %copy-start.3 = (f32[4]{0:T(128)S(1)}, f32[4]{0:T(128)}, u32[]{:S(2)}) copy-start(f32[4]{0:T(128)} %param.16) | copy-start | bytes 52
  7.4 55.9 %all-reduce.3.cloned.1.call-start = ((), (), s32[]{:S(2)}) async-start(), calls=%async_computation | async-start | bytes 3145728 | tf_op jit(solution)/shard_map/psum | solution.py:84
  8.3 22.3 %collective-permute-start.4 = (bf16[128,128]{1,0:T(8,128)(2,1)S(1)}, bf16[128,128]{1,0:T(8,128)(2,1)S(1)}, u32[]{:S(2)}, u32[]{:S(2)}) collective-permute-start(bf16[128,128]{1,0:T(8,128)(2,1)S(1)} %get-tuple-element.7), channel_id=1, source_target_pairs={{0,2},{2,4},{4,6},{6,8},{8,10},{10,12},{12,14},{14,16},{16,18},{18... | collective-permute-start | bytes 98312 | tf_op jit(solution)/shard_map/ppermute | solution.py:26
  13.2 17.4 %collective-permute-start.5 = (bf16[128,128]{1,0:T(8,128)(2,1)S(1)}, bf16[128,128]{1,0:T(8,128)(2,1)S(1)}, u32[]{:S(2)}, u32[]{:S(2)}) collective-permute-start(bf16[128,128]{1,0:T(8,128)(2,1)S(1)} %get-tuple-element.8), channel_id=1, source_target_pairs={{2,0},{4,2},{6,4},{8,6},{10,8},{12,10},{14,12},{16,14},{18,16},{20... | collective-permute-start | bytes 98312 | tf_op jit(solution)/shard_map/ppermute | solution.py:27
  15.2 11.9 %collective-permute-start.2 = (s32[128]{0:T(128)S(1)}, s32[128]{0:T(128)S(1)}, u32[]{:S(2)}, u32[]{:S(2)}) collective-permute-start(s32[128]{0:T(128)S(1)} %get-tuple-element.11), channel_id=1, source_target_pairs={{0,2},{2,4},{4,6},{6,8},{8,10},{10,12},{12,14},{14,16},{16,18},{18... | collective-permute-start | bytes 1544 | tf_op jit(solution)/shard_map/ppermute | solution.py:26
  19.8 8.7 %collective-permute-start.3 = (s32[128]{0:T(128)S(1)}, s32[128]{0:T(128)S(1)}, u32[]{:S(2)}, u32[]{:S(2)}) collective-permute-start(s32[128]{0:T(128)S(1)} %get-tuple-element.12), channel_id=1, source_target_pairs={{2,0},{4,2},{6,4},{8,6},{10,8},{12,10},{14,12},{16,14},{18,16},{20... | collective-permute-start | bytes 1544 | tf_op jit(solution)/shard_map/ppermute | solution.py:27
  22.2 11.4 %collective-permute-start = (bf16[128,128]{0,1:T(8,128)(2,1)S(1)}, bf16[128,128]{0,1:T(8,128)(2,1)S(1)}, u32[]{:S(2)}, u32[]{:S(2)}) collective-permute-start(bf16[128,128]{0,1:T(8,128)(2,1)S(1)} %get-tuple-element.9), channel_id=1, source_target_pairs={{0,2},{2,4},{4,6},{6,8},{8,10},{10,12},{12,14},{14,16},{16,18},{18... | collective-permute-start | bytes 98312 | tf_op jit(solution)/shard_map/ppermute | solution.py:26
  27.2 6.7 %collective-permute-start.1 = (bf16[128,128]{0,1:T(8,128)(2,1)S(1)}, bf16[128,128]{0,1:T(8,128)(2,1)S(1)}, u32[]{:S(2)}, u32[]{:S(2)}) collective-permute-start(bf16[128,128]{0,1:T(8,128)(2,1)S(1)} %get-tuple-element.10), channel_id=1, source_target_pairs={{2,0},{4,2},{6,4},{8,6},{10,8},{12,10},{14,12},{16,14},{18,16},{20... | collective-permute-start | bytes 98312 | tf_op jit(solution)/shard_map/ppermute | solution.py:27
  37.6 149.7 %all-gather.9.cloned.1.call-start = ((), (), s32[]{:S(2)}) async-start(), calls=%async_computation.4 | async-start | bytes 12255232 | tf_op jit(solution)/shard_map/all_gather | solution.py:15
  38.2 291.1 %all-gather.5.cloned.1.call-start = ((), (), s32[]{:S(2)}) async-start(), calls=%async_computation.1 | async-start | bytes 12255232 | tf_op jit(solution)/shard_map/all_gather | solution.py:96
  38.7 432.5 %all-gather.7.cloned.1.call-start = ((), (), s32[]{:S(2)}) async-start(), calls=%async_computation.2 | async-start | bytes 12255232 | tf_op jit(solution)/shard_map/all_gather | solution.py:97
  39.3 472.6 %all-reduce.5.cloned.1.call-start = ((), (), s32[]{:S(2)}) async-start(), calls=%async_computation.3 | async-start | bytes 3145728 | tf_op jit(solution)/shard_map/psum | solution.py:102
  66.0 263.3 %copy-start.2 = (bf16[384,2048]{1,0:T(8,128)(2,1)}, bf16[384,2048]{1,0:T(8,128)(2,1)S(1)}, u32[]{:S(2)}) copy-start(bf16[384,2048]{1,0:T(8,128)(2,1)S(1)} %get-tuple-element.6) | copy-start | bytes 4718596
  187.2 142.0 %copy-start.4 = (f32[2048]{0:T(1024)S(1)}, f32[2048]{0:T(1024)}, u32[]{:S(2)}) copy-start(f32[2048]{0:T(1024)} %param.18) | copy-start | bytes 24580
  471.3 44.3 %copy-start.1 = (bf16[512,2048]{1,0:T(8,128)(2,1)S(1)}, bf16[512,2048]{1,0:T(8,128)(2,1)}, u32[]{:S(2)}) copy-start(bf16[512,2048]{1,0:T(8,128)(2,1)} %param.17) | copy-start | bytes 6291460
Sparse Core Ops, SparseCore 0:
  37.7 25.5 all-reduce.2
  493.3 18.5 all-reduce.4
Sparse Core Ops, SparseCore 1:
  40.8 146.4 all-gather.8
  189.9 139.3 all-gather.4
  331.9 139.3 all-gather.6
